TPU v7x, 512 devices: a whole 4x4x16 slice. The times are simulated.
512 devices in a mesh: ra: 16 (over z), cb: 4 (over y), dp: 8 (over x, core).
Axes of the slice: x: 4, y: 4, z: 16, core: 2. Of those that a mesh axis runs over, the one named last changes fastest.
Arguments:
- tokens: bfloat16 [8, 512, 4096], P('dp', None, 'ra'), may hold values from -80 to 80
- pre_gain: float32 [4096], P('ra'), may hold values from 0.1 to 1.9
- w_gate: bfloat16 [4096, 11264], P('ra', 'cb'), may hold values from -0.09375 to 0.09375
- w_up: bfloat16 [4096, 11264], P('ra', 'cb'), may hold values from -0.09375 to 0.09375
- conv_gate: float32 [3, 11264], P(None, 'cb'), may hold values from -3.5 to 3.5
- conv_up: float32 [3, 11264], P(None, 'cb'), may hold values from -3.5 to 3.5
- w_down: bfloat16 [11264, 4096], P('cb', 'ra'), may hold values from -2 to 2
- post_gain: float32 [4096], P('ra'), may hold values from 0.1 to 1.9
Outputs:
- mixed: bfloat16 [8, 512, 4096], P('dp', None, 'ra')
All inputs are finite; a program needn't handle non-finite values.
Results may differ from a plain program's by a relative error of at most 0.0064.
Values may be sent and summed in bfloat16 or wider, within the bound.
A program may use at most 64 MiB of HBM per device.

v0:
```python
import jax
import jax.numpy as jnp
from jax import lax
from jax.sharding import PartitionSpec as P

epsilon = 1e-06
residual_scale = 0.125


def from_everyone(array, axis):
    count = lax.axis_size(axis)
    return lax.all_to_all(
        jnp.broadcast_to(array[None], (count, *array.shape)), axis, 0, 0, tiled=True
    )


def over_copies(array, axis):
    return from_everyone(array, axis).sum(axis=0)


def split_up(array, dim, count):
    dims = array.shape
    tiles = array.reshape(*dims[:dim], count, dims[dim] // count, *dims[dim + 1 :])
    return jnp.moveaxis(tiles, dim, 0)


def summed_on_arrival(array, axis, dim):
    count = lax.axis_size(axis)
    tiles = lax.all_to_all(split_up(array, dim, count), axis, 0, 0, tiled=True)
    return jnp.sum(tiles, axis=0)


def convolve(field, tap_weights):
    zero_col = jnp.zeros((field.shape[0], 1), jnp.float32)
    before = jnp.concatenate([zero_col, field[:, :-1]], axis=1)
    later_cols = jnp.concatenate([field[:, 1:], zero_col], axis=1)
    return (
        tap_weights[0][:, None] * before
        + tap_weights[1][:, None] * field
        + tap_weights[2][:, None] * later_cols
    )


def local(tokens, pre_gain, w_gate, w_up, conv_gate, conv_up, w_down, post_gain):
    ra_count = lax.axis_size("ra")
    dim_full = tokens.shape[2] * ra_count
    values = tokens[0].astype(jnp.float32)
    local_sq = jnp.sum(values * values, axis=1)
    total_sq = over_copies(local_sq, "ra")
    in_scale = lax.rsqrt(total_sq / dim_full + epsilon)
    weighted = (values * pre_gain).astype(jnp.bfloat16)
    gate_cols, up_cols = (
        lax.all_to_all(w_gate, "ra", split_axis=1, concat_axis=0, tiled=True),
        lax.all_to_all(w_up, "ra", split_axis=1, concat_axis=0, tiled=True),
    )
    own_units = gate_cols.shape[1]
    piece = lax.all_gather(weighted, "ra", axis=1, tiled=True)
    dims = (((0,), (1,)), ((), ()))
    gate_sum = lax.dot_general(gate_cols, piece, dims, preferred_element_type=jnp.float32)
    up_sum = lax.dot_general(up_cols, piece, dims, preferred_element_type=jnp.float32)
    offset_units = lax.axis_index("ra") * own_units
    taps_gate = lax.dynamic_slice_in_dim(conv_gate, offset_units, own_units, 1)
    taps_up = lax.dynamic_slice_in_dim(conv_up, offset_units, own_units, 1)
    gate_lin = gate_sum * in_scale[None, :]
    up_lin = up_sum * in_scale[None, :]
    hidden = (
        jax.nn.gelu(convolve(gate_lin, taps_gate), approximate=True) * convolve(up_lin, taps_up)
    ).astype(jnp.bfloat16)
    partial_value = lax.dot_general(
        lax.all_gather(hidden, "ra", axis=0, tiled=True),
        w_down,
        (((0,), (0,)), ((), ())),
        preferred_element_type=jnp.float32,
    )
    share = summed_on_arrival(partial_value, "cb", 1)
    share_cols = share.shape[1]
    col_start = lax.axis_index("cb") * share_cols
    own_values = lax.dynamic_slice_in_dim(values, col_start, share_cols, 1)
    own_gain = lax.dynamic_slice_in_dim(post_gain, col_start, share_cols, 0)
    post_sq = over_copies(jnp.sum(share * share, axis=1), ("ra", "cb"))
    post_scale = lax.rsqrt(post_sq / dim_full + epsilon)
    mixed_part = (residual_scale * own_values + share * post_scale[:, None] * own_gain).astype(
        jnp.bfloat16
    )
    mixed = lax.all_gather(mixed_part, "cb", axis=1, tiled=True)
    return mixed[None]


def solution(mesh):
    in_specs = (
        P("dp", None, "ra"),
        P("ra"),
        P("ra", "cb"),
        P("ra", "cb"),
        P(None, "cb"),
        P(None, "cb"),
        P("cb", "ra"),
        P("ra"),
    )
    out_specs = P("dp", None, "ra")
    return jax.shard_map(local, mesh=mesh, in_specs=in_specs, out_specs=out_specs, check_vma=False)
```

profile of v0, /device:TPU:2, one launch (start us, length us, event | category | flops | bytes accessed | tf_op | source)
XLA Modules:
  0.0 356.9 jit_solution(16461781965745227600)
XLA Ops:
  6.5 0.0 copy-start
  6.5 1.2 copy.25
  7.7 1.5 fusion.3
  9.2 0.6 broadcast_in_dim.6
  9.9 15.2 %all-to-all-start.1 = ((f32[16,1,512]{2,1,0:T(1,128)}), f32[16,1,512]{2,1,0:T(1,128)S(1)}, u32[]{:S(2)}, u32[]{:S(2)}) async-start(f32[16,1,512]{2,1,0:T(1,128)} %broadcast_in_dim.6), calls=%async_computation.1 | async-start | bytes 65536 | tf_op jit(solution)/shard_map/all_to_all | solution.py:12
  25.1 2.5 copy.29
  27.6 10.0 %all-to-all-done.1 = f32[16,1,512]{2,1,0:T(1,128)S(1)} async-done(((f32[16,1,512]{2,1,0:T(1,128)}), f32[16,1,512]{2,1,0:T(1,128)S(1)}, u32[]{:S(2)}, u32[]{:S(2)}) %all-to-all-start.1) | async-done | bytes 32800 | tf_op jit(solution)/shard_map/all_to_all | solution.py:12
  37.6 3.7 %all-to-all-start.2 = ((bf16[256,16,176]{0,2,1:T(8,128)(2,1)}), bf16[256,16,176]{0,2,1:T(8,128)(2,1)S(1)}, u32[]{:S(2)}, u32[]{:S(2)}) async-start(bf16[256,16,176]{0,2,1:T(8,128)(2,1)} %bitcast.41), calls=%async_computation.2 | async-start | bytes 2883584 | tf_op jit(solution)/shard_map/all_to_all | solution.py:54
  41.3 0.0 all-gather.3.cloned.1.call-start
  41.4 0.7 all-gather.3.cloned.1.call-update
  42.1 2.5 copy.26
  44.6 72.1 %all-to-all-done.2 = bf16[256,16,176]{0,2,1:T(8,128)(2,1)S(1)} async-done(((bf16[256,16,176]{0,2,1:T(8,128)(2,1)}), bf16[256,16,176]{0,2,1:T(8,128)(2,1)S(1)}, u32[]{:S(2)}, u32[]{:S(2)}) %all-to-all-start.2) | async-done | bytes 1441824 | tf_op jit(solution)/shard_map/all_to_all | solution.py:54
  116.7 10.3 %all-to-all-start = ((bf16[256,16,176]{0,2,1:T(8,128)(2,1)}), bf16[256,16,176]{0,2,1:T(8,128)(2,1)}, u32[]{:S(2)}, u32[]{:S(2)}) async-start(bf16[256,16,176]{0,2,1:T(8,128)(2,1)} %bitcast.40), calls=%async_computation | async-start | bytes 2883584 | tf_op jit(solution)/shard_map/all_to_all | solution.py:53
  127.0 0.0 all-gather.5.cloned.1.call-start
  127.1 0.9 constant_dynamic-slice_fusion
  128.0 1.3 copy.36
  129.3 78.8 %all-to-all-done = bf16[256,16,176]{0,2,1:T(8,128)(2,1)} async-done(((bf16[256,16,176]{0,2,1:T(8,128)(2,1)}), bf16[256,16,176]{0,2,1:T(8,128)(2,1)}, u32[]{:S(2)}, u32[]{:S(2)}) %all-to-all-start) | async-done | bytes 1441824 | tf_op jit(solution)/shard_map/all_to_all | solution.py:53
  208.2 0.0 copy-start.2
  208.2 2.8 copy.35
  210.9 5.6 %all-gather.3.cloned.1.call-done = bf16[512,4096]{0,1:T(8,128)(2,1)} async-done(((bf16[512,256]{0,1:T(8,128)(2,1)}), bf16[512,4096]{0,1:T(8,128)(2,1)}) %all-gather.3.cloned.1.call-update) | async-done | bytes 4194320 | tf_op jit(solution)/shard_map/all_gather | solution.py:57
  216.5 0.0 copy-done.2
  216.5 0.0 copy-start.1
  216.5 0.0 copy-start.3
  216.5 3.3 fusion.1
  219.8 0.2 copy-done.1
  220.0 0.4 copy-done.3
  220.4 0.9 fusion
  221.3 0.3 fusion.14
  221.6 1.2 fusion.12
  222.8 0.0 all-gather.5.cloned.1.call-update
  222.8 72.5 %all-gather.5.cloned.1.call-done = bf16[2816,512]{1,0:T(8,128)(2,1)} async-done(((bf16[176,512]{1,0:T(8,128)(2,1)}), bf16[2816,512]{1,0:T(8,128)(2,1)}) %all-gather.5.cloned.1.call-update) | async-done | bytes 2883600 | tf_op jit(solution)/shard_map/all_gather | solution.py:70
  295.4 0.0 copy-done
  295.4 2.8 fusion.16
  298.1 0.0 copy-start.4
  298.1 12.2 %all_to_all.55 = f32[4,512,64]{1,2,0:T(8,128)S(1)} all-to-all(f32[4,512,64]{1,2,0:T(8,128)S(1)} %bitcast.45), channel_id=1, replica_groups=mesh['ra'=16,'cb'=4,'dp'=8] {'cb'}, dimensions={0} | all-to-all | bytes 1048576 | tf_op jit(solution)/shard_map/all_to_all | solution.py:29
  310.4 0.7 broadcast_in_dim.7
  311.2 9.4 %all-to-all-start.4 = ((f32[64,1,512]{2,1,0:T(1,128)}), f32[64,1,512]{2,1,0:T(1,128)S(1)}, u32[]{:S(2)}, u32[]{:S(2)}) async-start(f32[64,1,512]{2,1,0:T(1,128)} %broadcast_in_dim.7), calls=%async_computation.4 | async-start | bytes 262144 | tf_op jit(solution)/shard_map/all_to_all | solution.py:12
  320.6 0.1 convert_element_type.15
  320.6 0.0 copy-done.4
  320.7 0.1 dynamic_slice.15
  320.7 16.0 %all-to-all-done.4 = f32[64,1,512]{2,1,0:T(1,128)S(1)} async-done(((f32[64,1,512]{2,1,0:T(1,128)}), f32[64,1,512]{2,1,0:T(1,128)S(1)}, u32[]{:S(2)}, u32[]{:S(2)}) %all-to-all-start.4) | async-done | bytes 131104 | tf_op jit(solution)/shard_map/all_to_all | solution.py:12
  336.7 0.1 reduce_sum.49
  336.8 0.1 fusion.13
  336.9 12.3 %all_gather.11 = bf16[512,256]{0,1:T(8,128)(2,1)S(1)} all-gather(bf16[512,64]{0,1:T(8,128)(2,1)S(1)} %fusion.13), channel_id=1, replica_groups=mesh['ra'=16,'cb'=4,'dp'=8] {'cb'}, dimensions={1}, use_global_device_ids=true | all-gather | bytes 327680 | tf_op jit(solution)/shard_map/all_gather | solution.py:85
  349.2 0.8 copy.32
  (5 shorter events, 0.1 us)
Async XLA Ops:
  6.5 288.8 %copy-start = (bf16[2816,256]{1,0:T(8,128)(2,1)S(1)}, bf16[2816,256]{1,0:T(8,128)(2,1)}, u32[]{:S(2)}) copy-start(bf16[2816,256]{1,0:T(8,128)(2,1)} %param.14) | copy-start | bytes 4325380
  9.9 27.8 %all-to-all-start.1 = ((f32[16,1,512]{2,1,0:T(1,128)}), f32[16,1,512]{2,1,0:T(1,128)S(1)}, u32[]{:S(2)}, u32[]{:S(2)}) async-start(f32[16,1,512]{2,1,0:T(1,128)} %broadcast_in_dim.6), calls=%async_computation.1 | async-start | bytes 65536 | tf_op jit(solution)/shard_map/all_to_all | solution.py:12
  37.6 79.1 %all-to-all-start.2 = ((bf16[256,16,176]{0,2,1:T(8,128)(2,1)}), bf16[256,16,176]{0,2,1:T(8,128)(2,1)S(1)}, u32[]{:S(2)}, u32[]{:S(2)}) async-start(bf16[256,16,176]{0,2,1:T(8,128)(2,1)} %bitcast.41), calls=%async_computation.2 | async-start | bytes 2883584 | tf_op jit(solution)/shard_map/all_to_all | solution.py:54
  41.3 175.2 %all-gather.3.cloned.1.call-start = ((), (), s32[]{:S(2)}) async-start(), calls=%async_computation.5 | async-start | bytes 4456448 | tf_op jit(solution)/shard_map/all_gather | solution.py:57
  116.7 91.4 %all-to-all-start = ((bf16[256,16,176]{0,2,1:T(8,128)(2,1)}), bf16[256,16,176]{0,2,1:T(8,128)(2,1)}, u32[]{:S(2)}, u32[]{:S(2)}) async-start(bf16[256,16,176]{0,2,1:T(8,128)(2,1)} %bitcast.40), calls=%async_computation | async-start | bytes 2883584 | tf_op jit(solution)/shard_map/all_to_all | solution.py:53
  127.0 168.3 %all-gather.5.cloned.1.call-start = ((), (), s32[]{:S(2)}) async-start(), calls=%async_computation.6 | async-start | bytes 3063808 | tf_op jit(solution)/shard_map/all_gather | solution.py:70
  208.2 8.4 %copy-start.2 = (bf16[16,22,8,256]{3,2,0,1:T(8,128)(2,1)S(1)}, bf16[16,22,8,256]{3,2,0,1:T(8,128)(2,1)}, u32[]{:S(2)}) copy-start(bf16[16,22,8,256]{3,2,0,1:T(8,128)(2,1)} %copy.36) | copy-start | bytes 4325380
  216.5 3.4 copy-start.1
  216.5 3.9 %copy-start.3 = (bf16[16,22,8,256]{3,2,0,1:T(8,128)(2,1)S(1)}, bf16[16,22,8,256]{3,2,0,1:T(8,128)(2,1)}, u32[]{:S(2)}) copy-start(bf16[16,22,8,256]{3,2,0,1:T(8,128)(2,1)} %copy.35) | copy-start | bytes 4325380
  298.1 22.5 %copy-start.4 = (f32[256]{0:T(256)S(1)}, f32[256]{0:T(256)}, u32[]{:S(2)}) copy-start(f32[256]{0:T(256)} %param.15) | copy-start | bytes 3076
  311.2 25.6 %all-to-all-start.4 = ((f32[64,1,512]{2,1,0:T(1,128)}), f32[64,1,512]{2,1,0:T(1,128)S(1)}, u32[]{:S(2)}, u32[]{:S(2)}) async-start(f32[64,1,512]{2,1,0:T(1,128)} %broadcast_in_dim.7), calls=%async_computation.4 | async-start | bytes 262144 | tf_op jit(solution)/shard_map/all_to_all | solution.py:12
Sparse Core Ops, SparseCore 0:
  44.2 172.2 all-gather.2
  222.9 72.3 all-gather.4
where the time goes:
time: 357 us
  waiting for transfers between devices  256 us (72%)
  starting transfers between devices  38.7 us (11%)
  blocking collectives  24.5 us (7%)
  local copies, waits for them, and re-layouts  14.4 us (4%)
  between operations  13.5 us (4%)
  matrix products  6.94 us (2%)
    all_to_all x1, waiting for transfers between devices, local(): lax.all_to_all(w_gate, 'ra', split_axis=1, concat_axis=0, tiled=True)  78.8 us
    all_gather x1, waiting for transfers between devices, local(): lax.all_gather(hidden, 'ra', axis=0, tiled=True)  72.5 us
    all_to_all x1, waiting for transfers between devices, local(): lax.all_to_all(w_up, 'ra', split_axis=1, concat_axis=0, tiled=True)  72.1 us
    all_to_all x2, waiting for transfers between devices, from_everyone(): lax.all_to_all(jnp.broadcast_to(array[None], (count, *array.shape)), axis...  26 us
    all_to_all x2, starting transfers between devices, from_everyone(): lax.all_to_all(jnp.broadcast_to(array[None], (count, *array.shape)), axis...  24.6 us
    all_gather x1, blocking collectives, local(): mixed = lax.all_gather(mixed_part, 'cb', axis=1, tiled=True)  12.3 us
    all_to_all x1, blocking collectives, summed_on_arrival(): tiles = lax.all_to_all(split_up(array, dim, count), axis, 0, 0, tiled=True)  12.2 us
    all_to_all x1, starting transfers between devices, local(): lax.all_to_all(w_gate, 'ra', split_axis=1, concat_axis=0, tiled=True)  10.3 us
  transfers between devices with their start and end apart: 6, of which 6 were waited for; matrix products, arithmetic and copies ran while one was open for 3% of the time, Pallas kernels for 0%

commit v1 on v0

--- a/solution.py
+++ b/solution.py
@@ -2,9 +2,16 @@
 import jax.numpy as jnp
 from jax import lax
 from jax.sharding import PartitionSpec as P
+from jax.lax import axis_index, axis_size, ppermute
 
 epsilon = 1e-06
 residual_scale = 0.125
+
+
+def tokens_play(w_in, where_dim):
+    z2 = list(w_in.shape[1:])
+    z2[where_dim] *= w_in.shape[0]
+    return jnp.moveaxis(w_in, 0, where_dim).reshape(z2)
 
 
 def from_everyone(array, axis):
@@ -42,6 +49,23 @@
 
 
 def local(tokens, pre_gain, w_gate, w_up, conv_gate, conv_up, w_down, post_gain):
+
+    def part_pairs_all_on_mesh(arr, named_axis, row_dim):
+        full_n = axis_size(named_axis)
+        buffer = [(at, (at + 1) % full_n) for at in range(full_n)]
+        inter, everything = ([], [])
+        pool = [(ix, m) for m, ix in buffer]
+        for w in range(full_n - 1):
+            if w % 2 == 0:
+                inter.append(ppermute(inter[-1] if inter else arr, named_axis, buffer))
+            else:
+                q_next = ppermute(everything[-1] if everything else arr, named_axis, perm=pool)
+                everything.append(q_next)
+        oldest = jnp.stack([*inter[::-1], arr, *everything])
+        y_new = axis_index(named_axis) - len(inter)
+        oldest = oldest[(jnp.arange(full_n) - y_new) % full_n]
+        return tokens_play(oldest, row_dim)
+
     ra_count = lax.axis_size("ra")
     dim_full = tokens.shape[2] * ra_count
     values = tokens[0].astype(jnp.float32)
@@ -67,7 +91,7 @@
         jax.nn.gelu(convolve(gate_lin, taps_gate), approximate=True) * convolve(up_lin, taps_up)
     ).astype(jnp.bfloat16)
     partial_value = lax.dot_general(
-        lax.all_gather(hidden, "ra", axis=0, tiled=True),
+        part_pairs_all_on_mesh(hidden, "ra", 0),
         w_down,
         (((0,), (0,)), ((), ())),
         preferred_element_type=jnp.float32,

time: 357 us -> 367 us (1.028)
  starting transfers between devices: 38.7 us -> 91.9 us
  waiting for transfers between devices: 256 us -> 204 us
  local copies, waits for them, and re-layouts: 14.4 us -> 22 us
    all_gather x1 -> x0, waiting for transfers between devices: 72.5 us -> none  [local(): lax.all_gather(hidden, 'ra', axis=0, tiled=True)]
    ppermute x0 -> x15, starting transfers between devices: none -> 52.7 us  [the longest x7 34.3 us: part_pairs_all_on_mesh(): ppermute(everything[-1] if everything else arr, named_axis, perm=pool)]
    ppermute x0 -> x15, waiting for transfers between devices: none -> 18.8 us  [the longest x8 17 us: part_pairs_all_on_mesh(): inter.append(ppermute(inter[-1] if inter else arr, named_axis, buffer))]
    unnamed x13 -> x59, local copies, waits for them, and re-layouts: 6.93 us -> 13.5 us
  transfers between devices with their start and end apart: 6 -> 20, of which waited for: 6 -> 15; matrix products, arithmetic and copies ran while one was open for 3% -> 4% of each run, Pallas kernels for 0% -> 0%
where the time goes in v1:
time: 367 us; the launch traced here: 366 us
  waiting for transfers between devices  204 us (56%)
  starting transfers between devices  91.9 us (25%)
  blocking collectives  24.5 us (7%)
  local copies, waits for them, and re-layouts  22 us (6%)
  between operations  14 us (4%)
  matrix products  7.29 us (2%)
    all_to_all x1, waiting for transfers between devices, local(): lax.all_to_all(w_gate, 'ra', split_axis=1, concat_axis=0, tiled=True)  78.7 us
    all_to_all x1, waiting for transfers between devices, local(): lax.all_to_all(w_up, 'ra', split_axis=1, concat_axis=0, tiled=True)  73.1 us
    ppermute x7, starting transfers between devices, part_pairs_all_on_mesh(): ppermute(everything[-1] if everything else arr, named_axis, perm=pool)  34.3 us
    all_to_all x2, waiting for transfers between devices, from_everyone(): lax.all_to_all(jnp.broadcast_to(array[None], (count, *array.shape)), axis...  25.9 us
    all_to_all x2, starting transfers between devices, from_everyone(): lax.all_to_all(jnp.broadcast_to(array[None], (count, *array.shape)), axis...  25.2 us
    ppermute x8, starting transfers between devices, part_pairs_all_on_mesh(): inter.append(ppermute(inter[-1] if inter else arr, named_axis, buffer))  18.4 us
    ppermute x8, waiting for transfers between devices, part_pairs_all_on_mesh(): inter.append(ppermute(inter[-1] if inter else arr, named_axis, buffer))  17 us
    unnamed x59, local copies, waits for them, and re-layouts  13.5 us
  transfers between devices with their start and end apart: 20, of which 15 were waited for; matrix products, arithmetic and copies ran while one was open for 4% of the time, Pallas kernels for 0%

profile of v1, /device:TPU:2, one launch (start us, length us, event | category | flops | bytes accessed | tf_op | source)
XLA Modules:
  0.0 366.4 jit_solution(5583362391558895906)
XLA Ops:
  6.5 1.1 copy.29
  7.6 1.5 fusion.3
  9.8 15.2 %all-to-all-start.1 = ((f32[16,1,512]{2,1,0:T(1,128)}), f32[16,1,512]{2,1,0:T(1,128)S(1)}, u32[]{:S(2)}, u32[]{:S(2)}) async-start(f32[16,1,512]{2,1,0:T(1,128)} %broadcast_in_dim.6), calls=%async_computation.1 | async-start | bytes 65536 | tf_op jit(solution)/shard_map/all_to_all | solution.py:19
  25.0 2.7 copy.33
  27.6 9.9 %all-to-all-done.1 = f32[16,1,512]{2,1,0:T(1,128)S(1)} async-done(((f32[16,1,512]{2,1,0:T(1,128)}), f32[16,1,512]{2,1,0:T(1,128)S(1)}, u32[]{:S(2)}, u32[]{:S(2)}) %all-to-all-start.1) | async-done | bytes 32800 | tf_op jit(solution)/shard_map/all_to_all | solution.py:19
  37.5 3.7 %all-to-all-start.2 = ((bf16[256,16,176]{0,2,1:T(8,128)(2,1)}), bf16[256,16,176]{0,2,1:T(8,128)(2,1)S(1)}, u32[]{:S(2)}, u32[]{:S(2)}) async-start(bf16[256,16,176]{0,2,1:T(8,128)(2,1)} %bitcast.9), calls=%async_computation.2 | async-start | bytes 2883584 | tf_op jit(solution)/shard_map/all_to_all | solution.py:78
  42.0 1.5 copy.30
  43.5 73.1 %all-to-all-done.2 = bf16[256,16,176]{0,2,1:T(8,128)(2,1)S(1)} async-done(((bf16[256,16,176]{0,2,1:T(8,128)(2,1)}), bf16[256,16,176]{0,2,1:T(8,128)(2,1)S(1)}, u32[]{:S(2)}, u32[]{:S(2)}) %all-to-all-start.2) | async-done | bytes 1441824 | tf_op jit(solution)/shard_map/all_to_all | solution.py:78
  116.6 10.2 %all-to-all-start = ((bf16[256,16,176]{0,2,1:T(8,128)(2,1)}), bf16[256,16,176]{0,2,1:T(8,128)(2,1)S(1)}, u32[]{:S(2)}, u32[]{:S(2)}) async-start(bf16[256,16,176]{0,2,1:T(8,128)(2,1)} %bitcast.3), calls=%async_computation | async-start | bytes 2883584 | tf_op jit(solution)/shard_map/all_to_all | solution.py:77
  127.8 1.4 copy.41
  129.2 78.7 %all-to-all-done = bf16[256,16,176]{0,2,1:T(8,128)(2,1)S(1)} async-done(((bf16[256,16,176]{0,2,1:T(8,128)(2,1)}), bf16[256,16,176]{0,2,1:T(8,128)(2,1)S(1)}, u32[]{:S(2)}, u32[]{:S(2)}) %all-to-all-start) | async-done | bytes 1441824 | tf_op jit(solution)/shard_map/all_to_all | solution.py:77
  207.9 1.3 copy.40
  209.3 7.2 %all-gather.2.cloned.1.call-done = bf16[512,4096]{0,1:T(8,128)(2,1)} async-done(((bf16[512,256]{0,1:T(8,128)(2,1)}), bf16[512,4096]{0,1:T(8,128)(2,1)}) %all-gather.2.cloned.1.call-update) | async-done | bytes 4194320 | tf_op jit(solution)/shard_map/all_gather | solution.py:81
  216.4 3.3 fusion.1
  222.0 3.5 collective-permute-start
  225.5 5.1 %collective-permute-done = bf16[176,512]{1,0:T(8,128)(2,1)S(1)} collective-permute-done((bf16[176,512]{1,0:T(8,128)(2,1)S(1)}, bf16[176,512]{1,0:T(8,128)(2,1)S(1)}, u32[]{:S(2)}, u32[]{:S(2)}) %collective-permute-start) | collective-permute-done | bytes 180256 | tf_op jit(solution)/shard_map/ppermute | solution.py:60
  230.6 2.2 collective-permute-start.1
  232.9 4.8 %collective-permute-start.8 = (bf16[176,512]{1,0:T(8,128)(2,1)S(1)}, bf16[176,512]{1,0:T(8,128)(2,1)S(1)}, u32[]{:S(2)}, u32[]{:S(2)}) collective-permute-start(bf16[176,512]{1,0:T(8,128)(2,1)S(1)} %fusion.12), channel_id=1, source_target_pairs={{32,0},{64,32},{96,64},{128,96},{160,128},{192,160},{224,192},{256... | collective-permute-start | bytes 540680 | tf_op jit(solution)/shard_map/ppermute | solution.py:62
  237.7 1.5 collective-permute-done.1
  239.2 2.8 collective-permute-start.2
  242.0 4.2 %collective-permute-start.9 = (bf16[176,512]{1,0:T(8,128)(2,1)S(1)}, bf16[176,512]{1,0:T(8,128)(2,1)S(1)}, u32[]{:S(2)}, u32[]{:S(2)}) collective-permute-start(bf16[176,512]{1,0:T(8,128)(2,1)S(1)} %collective-permute-done.8), channel_id=1, source_target_pairs={{32,0},{64,32},{96,64},{128,96},{160,128},{192,160},{224,192},{256... | collective-permute-start | bytes 540680 | tf_op jit(solution)/shard_map/ppermute | solution.py:62
  246.3 2.3 collective-permute-done.2
  248.6 2.2 collective-permute-start.3
  251.6 4.3 %collective-permute-start.10 = (bf16[176,512]{1,0:T(8,128)(2,1)S(1)}, bf16[176,512]{1,0:T(8,128)(2,1)S(1)}, u32[]{:S(2)}, u32[]{:S(2)}) collective-permute-start(bf16[176,512]{1,0:T(8,128)(2,1)S(1)} %collective-permute-done.9), channel_id=1, source_target_pairs={{32,0},{64,32},{96,64},{128,96},{160,128},{192,160},{224,192},{256... | collective-permute-start | bytes 540680 | tf_op jit(solution)/shard_map/ppermute | solution.py:62
  255.9 3.2 collective-permute-done.3
  259.1 1.9 collective-permute-start.4
  261.0 5.1 %collective-permute-start.11 = (bf16[176,512]{1,0:T(8,128)(2,1)S(1)}, bf16[176,512]{1,0:T(8,128)(2,1)S(1)}, u32[]{:S(2)}, u32[]{:S(2)}) collective-permute-start(bf16[176,512]{1,0:T(8,128)(2,1)S(1)} %collective-permute-done.10), channel_id=1, source_target_pairs={{32,0},{64,32},{96,64},{128,96},{160,128},{192,160},{224,192},{256... | collective-permute-start | bytes 540680 | tf_op jit(solution)/shard_map/ppermute | solution.py:62
  266.2 2.6 collective-permute-done.4
  268.8 1.9 collective-permute-start.5
  270.7 5.1 %collective-permute-start.12 = (bf16[176,512]{1,0:T(8,128)(2,1)S(1)}, bf16[176,512]{1,0:T(8,128)(2,1)S(1)}, u32[]{:S(2)}, u32[]{:S(2)}) collective-permute-start(bf16[176,512]{1,0:T(8,128)(2,1)S(1)} %collective-permute-done.11), channel_id=1, source_target_pairs={{32,0},{64,32},{96,64},{128,96},{160,128},{192,160},{224,192},{256... | collective-permute-start | bytes 540680 | tf_op jit(solution)/shard_map/ppermute | solution.py:62
  275.8 2.0 collective-permute-done.5
  277.9 1.9 collective-permute-start.6
  279.8 1.7 copy.35
  281.5 5.1 %collective-permute-start.13 = (bf16[176,512]{1,0:T(8,128)(2,1)S(1)}, bf16[176,512]{1,0:T(8,128)(2,1)S(1)}, u32[]{:S(2)}, u32[]{:S(2)}) collective-permute-start(bf16[176,512]{1,0:T(8,128)(2,1)S(1)} %collective-permute-done.12), channel_id=1, source_target_pairs={{32,0},{64,32},{96,64},{128,96},{160,128},{192,160},{224,192},{256... | collective-permute-start | bytes 540680 | tf_op jit(solution)/shard_map/ppermute | solution.py:62
  286.8 1.9 collective-permute-start.7
  288.7 1.1 collective-permute-done.13
  289.8 5.6 %collective-permute-start.14 = (bf16[176,512]{1,0:T(8,128)(2,1)S(1)}, bf16[176,512]{1,0:T(8,128)(2,1)S(1)}, u32[]{:S(2)}, u32[]{:S(2)}) collective-permute-start(bf16[176,512]{1,0:T(8,128)(2,1)S(1)} %collective-permute-done.13), channel_id=1, source_target_pairs={{32,0},{64,32},{96,64},{128,96},{160,128},{192,160},{224,192},{256... | collective-permute-start | bytes 540680 | tf_op jit(solution)/shard_map/ppermute | solution.py:62
  295.6 1.0 bitcast_dynamic-update-slice_fusion.14
  296.6 0.9 bitcast_dynamic-update-slice_fusion.13
  297.6 0.9 bitcast_dynamic-update-slice_fusion.12
  298.5 0.9 bitcast_dynamic-update-slice_fusion.11
  299.4 0.9 bitcast_dynamic-update-slice_fusion.10
  301.6 2.3 gather_fusion
  303.9 3.1 convolution_bitcast_fusion
  307.0 12.2 %all_to_all.55 = f32[4,512,64]{1,2,0:T(8,128)S(1)} all-to-all(f32[4,512,64]{1,2,0:T(8,128)S(1)} %convolution_bitcast_fusion), channel_id=1, replica_groups=mesh['ra'=16,'cb'=4,'dp'=8] {'cb'}, dimensions={0} | all-to-all | bytes 1048576 | tf_op jit(solution)/shard_map/all_to_all | solution.py:36
  320.1 10.0 %all-to-all-start.4 = ((f32[64,1,512]{2,1,0:T(1,128)}), f32[64,1,512]{2,1,0:T(1,128)S(1)}, u32[]{:S(2)}, u32[]{:S(2)}) async-start(f32[64,1,512]{2,1,0:T(1,128)} %broadcast_in_dim.7), calls=%async_computation.4 | async-start | bytes 262144 | tf_op jit(solution)/shard_map/all_to_all | solution.py:19
  330.2 16.0 %all-to-all-done.4 = f32[64,1,512]{2,1,0:T(1,128)S(1)} async-done(((f32[64,1,512]{2,1,0:T(1,128)}), f32[64,1,512]{2,1,0:T(1,128)S(1)}, u32[]{:S(2)}, u32[]{:S(2)}) %all-to-all-start.4) | async-done | bytes 131104 | tf_op jit(solution)/shard_map/all_to_all | solution.py:19
  346.5 12.3 %all_gather.7 = bf16[512,256]{0,1:T(8,128)(2,1)S(1)} all-gather(bf16[512,64]{0,1:T(8,128)(2,1)S(1)} %fusion.13), channel_id=1, replica_groups=mesh['ra'=16,'cb'=4,'dp'=8] {'cb'}, dimensions={1}, use_global_device_ids=true | all-gather | bytes 327680 | tf_op jit(solution)/shard_map/all_gather | solution.py:109
  (79 shorter events, 8.8 us)
Async XLA Ops:
  9.8 27.8 %all-to-all-start.1 = ((f32[16,1,512]{2,1,0:T(1,128)}), f32[16,1,512]{2,1,0:T(1,128)S(1)}, u32[]{:S(2)}, u32[]{:S(2)}) async-start(f32[16,1,512]{2,1,0:T(1,128)} %broadcast_in_dim.6), calls=%async_computation.1 | async-start | bytes 65536 | tf_op jit(solution)/shard_map/all_to_all | solution.py:19
  25.0 17.0 %copy-start.3 = (bf16[256,2816]{1,0:T(8,128)(2,1)S(1)}, bf16[256,2816]{1,0:T(8,128)(2,1)}, u32[]{:S(2)}) copy-start(bf16[256,2816]{1,0:T(8,128)(2,1)} %param.10) | copy-start | bytes 4325380
  37.5 79.1 %all-to-all-start.2 = ((bf16[256,16,176]{0,2,1:T(8,128)(2,1)}), bf16[256,16,176]{0,2,1:T(8,128)(2,1)S(1)}, u32[]{:S(2)}, u32[]{:S(2)}) async-start(bf16[256,16,176]{0,2,1:T(8,128)(2,1)} %bitcast.9), calls=%async_computation.2 | async-start | bytes 2883584 | tf_op jit(solution)/shard_map/all_to_all | solution.py:78
  41.2 175.2 %all-gather.2.cloned.1.call-start = ((), (), s32[]{:S(2)}) async-start(), calls=%async_computation.5 | async-start | bytes 4456448 | tf_op jit(solution)/shard_map/all_gather | solution.py:81
  116.6 91.3 %all-to-all-start = ((bf16[256,16,176]{0,2,1:T(8,128)(2,1)}), bf16[256,16,176]{0,2,1:T(8,128)(2,1)S(1)}, u32[]{:S(2)}, u32[]{:S(2)}) async-start(bf16[256,16,176]{0,2,1:T(8,128)(2,1)} %bitcast.3), calls=%async_computation | async-start | bytes 2883584 | tf_op jit(solution)/shard_map/all_to_all | solution.py:77
  129.2 87.2 %copy-start.1 = (bf16[16,22,8,256]{3,2,0,1:T(8,128)(2,1)S(1)}, bf16[16,22,8,256]{3,2,0,1:T(8,128)(2,1)}, u32[]{:S(2)}) copy-start(bf16[16,22,8,256]{3,2,0,1:T(8,128)(2,1)} %copy.41) | copy-start | bytes 4325380
  216.4 3.4 copy-start
  216.4 3.9 %copy-start.2 = (bf16[16,22,8,256]{3,2,0,1:T(8,128)(2,1)S(1)}, bf16[16,22,8,256]{3,2,0,1:T(8,128)(2,1)}, u32[]{:S(2)}) copy-start(bf16[16,22,8,256]{3,2,0,1:T(8,128)(2,1)} %copy.40) | copy-start | bytes 4325380
  221.2 58.6 %copy-start.4 = (bf16[2816,256]{1,0:T(8,128)(2,1)S(1)}, bf16[2816,256]{1,0:T(8,128)(2,1)}, u32[]{:S(2)}) copy-start(bf16[2816,256]{1,0:T(8,128)(2,1)} %param.14) | copy-start | bytes 4325380
  222.0 8.6 %collective-permute-start = (bf16[176,512]{1,0:T(8,128)(2,1)S(1)}, bf16[176,512]{1,0:T(8,128)(2,1)S(1)}, u32[]{:S(2)}, u32[]{:S(2)}) collective-permute-start(bf16[176,512]{1,0:T(8,128)(2,1)S(1)} %fusion.12), channel_id=1, source_target_pairs={{0,32},{32,64},{64,96},{96,128},{128,160},{160,192},{192,224},{224... | collective-permute-start | bytes 540680 | tf_op jit(solution)/shard_map/ppermute | solution.py:60
  230.6 8.6 %collective-permute-start.1 = (bf16[176,512]{1,0:T(8,128)(2,1)S(1)}, bf16[176,512]{1,0:T(8,128)(2,1)S(1)}, u32[]{:S(2)}, u32[]{:S(2)}) collective-permute-start(bf16[176,512]{1,0:T(8,128)(2,1)S(1)} %collective-permute-done), channel_id=1, source_target_pairs={{0,32},{32,64},{64,96},{96,128},{128,160},{160,192},{192,224},{224... | collective-permute-start | bytes 540680 | tf_op jit(solution)/shard_map/ppermute | solution.py:60
  232.9 9.2 %collective-permute-start.8 = (bf16[176,512]{1,0:T(8,128)(2,1)S(1)}, bf16[176,512]{1,0:T(8,128)(2,1)S(1)}, u32[]{:S(2)}, u32[]{:S(2)}) collective-permute-start(bf16[176,512]{1,0:T(8,128)(2,1)S(1)} %fusion.12), channel_id=1, source_target_pairs={{32,0},{64,32},{96,64},{128,96},{160,128},{192,160},{224,192},{256... | collective-permute-start | bytes 540680 | tf_op jit(solution)/shard_map/ppermute | solution.py:62
  239.2 56.2 %copy-start.7 = (bf16[176,512]{1,0:T(8,128)(2,1)}, bf16[176,512]{1,0:T(8,128)(2,1)S(1)}, u32[]{:S(2)}) copy-start(bf16[176,512]{1,0:T(8,128)(2,1)S(1)} %collective-permute-done.1) | copy-start | bytes 540676
  239.2 9.4 %collective-permute-start.2 = (bf16[176,512]{1,0:T(8,128)(2,1)S(1)}, bf16[176,512]{1,0:T(8,128)(2,1)S(1)}, u32[]{:S(2)}, u32[]{:S(2)}) collective-permute-start(bf16[176,512]{1,0:T(8,128)(2,1)S(1)} %collective-permute-done.1), channel_id=1, source_target_pairs={{0,32},{32,64},{64,96},{96,128},{128,160},{160,192},{192,224},{224... | collective-permute-start | bytes 540680 | tf_op jit(solution)/shard_map/ppermute | solution.py:60
  242.0 53.4 %copy-start.5 = (bf16[176,512]{1,0:T(8,128)(2,1)}, bf16[176,512]{1,0:T(8,128)(2,1)S(1)}, u32[]{:S(2)}) copy-start(bf16[176,512]{1,0:T(8,128)(2,1)S(1)} %collective-permute-done.8) | copy-start | bytes 540676
  242.0 9.6 %collective-permute-start.9 = (bf16[176,512]{1,0:T(8,128)(2,1)S(1)}, bf16[176,512]{1,0:T(8,128)(2,1)S(1)}, u32[]{:S(2)}, u32[]{:S(2)}) collective-permute-start(bf16[176,512]{1,0:T(8,128)(2,1)S(1)} %collective-permute-done.8), channel_id=1, source_target_pairs={{32,0},{64,32},{96,64},{128,96},{160,128},{192,160},{224,192},{256... | collective-permute-start | bytes 540680 | tf_op jit(solution)/shard_map/ppermute | solution.py:62
  248.6 46.8 %copy-start.10 = (bf16[176,512]{1,0:T(8,128)(2,1)}, bf16[176,512]{1,0:T(8,128)(2,1)S(1)}, u32[]{:S(2)}) copy-start(bf16[176,512]{1,0:T(8,128)(2,1)S(1)} %collective-permute-done.2) | copy-start | bytes 540676
  248.6 10.5 %collective-permute-start.3 = (bf16[176,512]{1,0:T(8,128)(2,1)S(1)}, bf16[176,512]{1,0:T(8,128)(2,1)S(1)}, u32[]{:S(2)}, u32[]{:S(2)}) collective-permute-start(bf16[176,512]{1,0:T(8,128)(2,1)S(1)} %collective-permute-done.2), channel_id=1, source_target_pairs={{0,32},{32,64},{64,96},{96,128},{128,160},{160,192},{192,224},{224... | collective-permute-start | bytes 540680 | tf_op jit(solution)/shard_map/ppermute | solution.py:60
  251.6 43.8 %copy-start.8 = (bf16[176,512]{1,0:T(8,128)(2,1)}, bf16[176,512]{1,0:T(8,128)(2,1)S(1)}, u32[]{:S(2)}) copy-start(bf16[176,512]{1,0:T(8,128)(2,1)S(1)} %collective-permute-done.9) | copy-start | bytes 540676
  251.6 9.4 %collective-permute-start.10 = (bf16[176,512]{1,0:T(8,128)(2,1)S(1)}, bf16[176,512]{1,0:T(8,128)(2,1)S(1)}, u32[]{:S(2)}, u32[]{:S(2)}) collective-permute-start(bf16[176,512]{1,0:T(8,128)(2,1)S(1)} %collective-permute-done.9), channel_id=1, source_target_pairs={{32,0},{64,32},{96,64},{128,96},{160,128},{192,160},{224,192},{256... | collective-permute-start | bytes 540680 | tf_op jit(solution)/shard_map/ppermute | solution.py:62
  259.1 36.3 %copy-start.15 = (bf16[176,512]{1,0:T(8,128)(2,1)}, bf16[176,512]{1,0:T(8,128)(2,1)S(1)}, u32[]{:S(2)}) copy-start(bf16[176,512]{1,0:T(8,128)(2,1)S(1)} %collective-permute-done.3) | copy-start | bytes 540676
  259.1 9.7 %collective-permute-start.4 = (bf16[176,512]{1,0:T(8,128)(2,1)S(1)}, bf16[176,512]{1,0:T(8,128)(2,1)S(1)}, u32[]{:S(2)}, u32[]{:S(2)}) collective-permute-start(bf16[176,512]{1,0:T(8,128)(2,1)S(1)} %collective-permute-done.3), channel_id=1, source_target_pairs={{0,32},{32,64},{64,96},{96,128},{128,160},{160,192},{192,224},{224... | collective-permute-start | bytes 540680 | tf_op jit(solution)/shard_map/ppermute | solution.py:60
  261.0 34.4 %copy-start.11 = (bf16[176,512]{1,0:T(8,128)(2,1)}, bf16[176,512]{1,0:T(8,128)(2,1)S(1)}, u32[]{:S(2)}) copy-start(bf16[176,512]{1,0:T(8,128)(2,1)S(1)} %collective-permute-done.10) | copy-start | bytes 540676
  261.0 9.7 %collective-permute-start.11 = (bf16[176,512]{1,0:T(8,128)(2,1)S(1)}, bf16[176,512]{1,0:T(8,128)(2,1)S(1)}, u32[]{:S(2)}, u32[]{:S(2)}) collective-permute-start(bf16[176,512]{1,0:T(8,128)(2,1)S(1)} %collective-permute-done.10), channel_id=1, source_target_pairs={{32,0},{64,32},{96,64},{128,96},{160,128},{192,160},{224,192},{256... | collective-permute-start | bytes 540680 | tf_op jit(solution)/shard_map/ppermute | solution.py:62
  268.7 1.9 copy-start.18
  268.8 9.1 %collective-permute-start.5 = (bf16[176,512]{1,0:T(8,128)(2,1)S(1)}, bf16[176,512]{1,0:T(8,128)(2,1)}, u32[]{:S(2)}, u32[]{:S(2)}) collective-permute-start(bf16[176,512]{1,0:T(8,128)(2,1)S(1)} %collective-permute-done.4), channel_id=1, source_target_pairs={{0,32},{32,64},{64,96},{96,128},{128,160},{160,192},{192,224},{224... | collective-permute-start | bytes 540680 | tf_op jit(solution)/shard_map/ppermute | solution.py:60
  270.7 24.8 %copy-start.13 = (bf16[176,512]{1,0:T(8,128)(2,1)}, bf16[176,512]{1,0:T(8,128)(2,1)S(1)}, u32[]{:S(2)}) copy-start(bf16[176,512]{1,0:T(8,128)(2,1)S(1)} %collective-permute-done.11) | copy-start | bytes 540676
  270.7 10.8 %collective-permute-start.12 = (bf16[176,512]{1,0:T(8,128)(2,1)S(1)}, bf16[176,512]{1,0:T(8,128)(2,1)S(1)}, u32[]{:S(2)}, u32[]{:S(2)}) collective-permute-start(bf16[176,512]{1,0:T(8,128)(2,1)S(1)} %collective-permute-done.11), channel_id=1, source_target_pairs={{32,0},{64,32},{96,64},{128,96},{160,128},{192,160},{224,192},{256... | collective-permute-start | bytes 540680 | tf_op jit(solution)/shard_map/ppermute | solution.py:62
  277.9 8.9 %collective-permute-start.6 = (bf16[176,512]{1,0:T(8,128)(2,1)}, bf16[176,512]{1,0:T(8,128)(2,1)}, u32[]{:S(2)}, u32[]{:S(2)}) collective-permute-start(bf16[176,512]{1,0:T(8,128)(2,1)} %collective-permute-done.5), channel_id=1, source_target_pairs={{0,32},{32,64},{64,96},{96,128},{128,160},{160,192},{192,224},{224... | collective-permute-start | bytes 540680 | tf_op jit(solution)/shard_map/ppermute | solution.py:60
  281.5 13.9 %copy-start.16 = (bf16[176,512]{1,0:T(8,128)(2,1)}, bf16[176,512]{1,0:T(8,128)(2,1)S(1)}, u32[]{:S(2)}) copy-start(bf16[176,512]{1,0:T(8,128)(2,1)S(1)} %collective-permute-done.12) | copy-start | bytes 540676
  281.5 8.3 %collective-permute-start.13 = (bf16[176,512]{1,0:T(8,128)(2,1)S(1)}, bf16[176,512]{1,0:T(8,128)(2,1)S(1)}, u32[]{:S(2)}, u32[]{:S(2)}) collective-permute-start(bf16[176,512]{1,0:T(8,128)(2,1)S(1)} %collective-permute-done.12), channel_id=1, source_target_pairs={{32,0},{64,32},{96,64},{128,96},{160,128},{192,160},{224,192},{256... | collective-permute-start | bytes 540680 | tf_op jit(solution)/shard_map/ppermute | solution.py:62
  286.8 8.8 %collective-permute-start.7 = (bf16[176,512]{1,0:T(8,128)(2,1)}, bf16[176,512]{1,0:T(8,128)(2,1)S(1)}, u32[]{:S(2)}, u32[]{:S(2)}) collective-permute-start(bf16[176,512]{1,0:T(8,128)(2,1)} %collective-permute-done.6), channel_id=1, source_target_pairs={{0,32},{32,64},{64,96},{96,128},{128,160},{160,192},{192,224},{224... | collective-permute-start | bytes 540680 | tf_op jit(solution)/shard_map/ppermute | solution.py:60
  289.8 11.8 %collective-permute-start.14 = (bf16[176,512]{1,0:T(8,128)(2,1)S(1)}, bf16[176,512]{1,0:T(8,128)(2,1)S(1)}, u32[]{:S(2)}, u32[]{:S(2)}) collective-permute-start(bf16[176,512]{1,0:T(8,128)(2,1)S(1)} %collective-permute-done.13), channel_id=1, source_target_pairs={{32,0},{64,32},{96,64},{128,96},{160,128},{192,160},{224,192},{256... | collective-permute-start | bytes 540680 | tf_op jit(solution)/shard_map/ppermute | solution.py:62
  295.6 5.8 %copy-start.6 = (bf16[176,512]{1,0:T(8,128)(2,1)S(1)}, bf16[176,512]{1,0:T(8,128)(2,1)}, u32[]{:S(2)}) copy-start(bf16[176,512]{1,0:T(8,128)(2,1)} %copy-done.5) | copy-start | bytes 540676
  295.6 5.8 %copy-start.9 = (bf16[176,512]{1,0:T(8,128)(2,1)S(1)}, bf16[176,512]{1,0:T(8,128)(2,1)}, u32[]{:S(2)}) copy-start(bf16[176,512]{1,0:T(8,128)(2,1)} %copy-done.8) | copy-start | bytes 540676
  295.6 5.9 %copy-start.12 = (bf16[176,512]{1,0:T(8,128)(2,1)S(1)}, bf16[176,512]{1,0:T(8,128)(2,1)}, u32[]{:S(2)}) copy-start(bf16[176,512]{1,0:T(8,128)(2,1)} %copy-done.11) | copy-start | bytes 540676
  295.6 5.9 %copy-start.14 = (bf16[176,512]{1,0:T(8,128)(2,1)S(1)}, bf16[176,512]{1,0:T(8,128)(2,1)}, u32[]{:S(2)}) copy-start(bf16[176,512]{1,0:T(8,128)(2,1)} %copy-done.13) | copy-start | bytes 540676
  295.6 5.9 %copy-start.17 = (bf16[176,512]{1,0:T(8,128)(2,1)S(1)}, bf16[176,512]{1,0:T(8,128)(2,1)}, u32[]{:S(2)}) copy-start(bf16[176,512]{1,0:T(8,128)(2,1)} %copy-done.16) | copy-start | bytes 540676
  307.0 23.1 %copy-start.19 = (f32[256]{0:T(256)S(1)}, f32[256]{0:T(256)}, u32[]{:S(2)}) copy-start(f32[256]{0:T(256)} %param.15) | copy-start | bytes 3076
  320.1 26.2 %all-to-all-start.4 = ((f32[64,1,512]{2,1,0:T(1,128)}), f32[64,1,512]{2,1,0:T(1,128)S(1)}, u32[]{:S(2)}, u32[]{:S(2)}) async-start(f32[64,1,512]{2,1,0:T(1,128)} %broadcast_in_dim.7), calls=%async_computation.4 | async-start | bytes 262144 | tf_op jit(solution)/shard_map/all_to_all | solution.py:19
Sparse Core Ops, SparseCore 0:
  44.1 172.2 all-gather.1
